TPU v7x, 512 devices: a whole 4x4x16 slice. The times are simulated.
512 devices in a mesh: dp: 4 (over x), kv: 64 (over z, y), tp: 2 (over core).
Axes of the slice: x: 4, y: 4, z: 16, core: 2. Of those that a mesh axis runs over, the one named last changes fastest.
Arguments:
- tokens: bfloat16 [4, 20480, 2048], P('dp', 'kv'), may hold values from -72 to 72
- w_query: bfloat16 [2048, 512], P(None, 'tp'), may hold values from -0.125 to 0.125
- key_weight: bfloat16 [2048, 256], P(None, 'tp'), may hold values from -0.125 to 0.125
- value_weight: bfloat16 [2048, 256], P(None, 'tp'), may hold values from -2.09375 to 2.09375
- w_out: bfloat16 [512, 2048], P(None, 'tp'), may hold values from -0.25 to 0.25
- chosen: int32 [4, 640, 16], P('dp', 'kv'), may hold values from -1 to 639, as said below
Outputs:
- mixed: bfloat16 [4, 20480, 2048], P('dp', 'kv', 'tp')
- log_mass: float32 [4, 4, 20480], P('dp', 'tp', 'kv')
Inputs may be any that keep to these rules, and one draw needn't show every extreme that they name: `chosen`: entry 0 of row i of a sequence is i; the other entries are distinct blocks before i, or -1 for an empty slot. The 10 rows of one index of kv together name at most one block held by any other index of kv; this bound is reached.
All inputs are finite; a program needn't handle non-finite values.
Results may differ from a plain program's by a relative error of at most 0.006.
The roundings to bfloat16 on the way count: a program that leaves them out, or rounds other values in their place, can miss the bound.
Values may be sent and summed in bfloat16 or wider, within the bound.
A program may use at most 64 MiB of HBM per device.

v0:
```python
import jax
import jax.numpy as jnp
from jax import lax
from jax.sharding import PartitionSpec as P

HEAD_WIDTH = 128


def body(tokens, w_query, key_weight, value_weight, w_out, chosen):
    local_tokens = tokens[0]
    local_chosen = chosen[0]
    row_count = local_tokens.shape[0]
    blocks_here, select_count = local_chosen.shape
    block_rows = row_count // blocks_here
    kv_heads = key_weight.shape[1] // HEAD_WIDTH
    query_heads = w_query.shape[1] // HEAD_WIDTH
    heads_per_group = query_heads // kv_heads
    width_kv = kv_heads * HEAD_WIDTH
    devices = lax.axis_size("kv")
    my_index = lax.axis_index("kv")
    queries = jnp.dot(local_tokens, w_query, preferred_element_type=jnp.float32).astype(
        jnp.bfloat16
    )
    projected_keys = jnp.dot(local_tokens, key_weight, preferred_element_type=jnp.float32).astype(
        jnp.bfloat16
    )
    projected_values = jnp.dot(
        local_tokens, value_weight, preferred_element_type=jnp.float32
    ).astype(jnp.bfloat16)
    paired = jnp.concatenate([projected_keys, projected_values], axis=1)
    owners = local_chosen // blocks_here
    inner_ix = local_chosen % blocks_here
    remote = (local_chosen >= 0) & (owners != my_index)
    peer_ids = jnp.arange(devices, dtype=jnp.int32)
    requests = jnp.where(
        remote[..., None] & (owners[..., None] == peer_ids), inner_ix[..., None], -1
    )
    wanted = jnp.max(requests, axis=(0, 1)).reshape(devices, 1)
    asked_ids = lax.all_to_all(wanted, "kv", split_axis=0, concat_axis=0, tiled=True)
    own_blocks = paired.reshape(blocks_here, block_rows, 2 * width_kv)
    replies = jnp.take(own_blocks, jnp.maximum(asked_ids[:, 0], 0), axis=0)
    arrived = lax.all_to_all(replies, "kv", split_axis=0, concat_axis=0, tiled=True)
    block_table = jnp.concatenate([arrived, own_blocks], axis=0)
    lookup = jnp.where(remote, owners, devices + inner_ix)
    picked = jnp.take(block_table, lookup, axis=0)
    selected_keys = picked[..., :width_kv].reshape(
        blocks_here, select_count * block_rows, kv_heads, HEAD_WIDTH
    )
    selected_values = picked[..., width_kv:].reshape(
        blocks_here, select_count * block_rows, kv_heads, HEAD_WIDTH
    )
    grouped_queries = queries.reshape(
        blocks_here, block_rows, kv_heads, heads_per_group, HEAD_WIDTH
    )
    scores = jnp.einsum(
        "btkgd,bskd->bkgts", grouped_queries, selected_keys, preferred_element_type=jnp.float32
    ) * HEAD_WIDTH ** (-0.5)
    bounded_index = jnp.maximum(local_chosen, 0)
    key_pos = (
        bounded_index[..., None] * block_rows + jnp.arange(block_rows, dtype=jnp.int32)
    ).reshape(blocks_here, select_count * block_rows)
    key_live = jnp.repeat(local_chosen >= 0, block_rows, axis=1)
    block_ids = my_index * blocks_here + jnp.arange(blocks_here, dtype=jnp.int32)
    query_pos = block_ids[:, None] * block_rows + jnp.arange(block_rows, dtype=jnp.int32)[None, :]
    allowed = key_live[:, None, :] & (key_pos[:, None, :] <= query_pos[:, :, None])
    scores = jnp.where(allowed[:, None, None], scores, -jnp.inf)
    row_max = jnp.max(scores, axis=-1)
    weights = jnp.exp(scores - row_max[..., None])
    row_sum = jnp.sum(weights, axis=-1)
    probs_low = weights.astype(jnp.bfloat16)
    summed = jnp.einsum(
        "bkgts,bskd->btkgd", probs_low, selected_values, preferred_element_type=jnp.float32
    )
    attended = (
        (summed / row_sum.transpose(0, 3, 1, 2)[..., None])
        .astype(jnp.bfloat16)
        .reshape(row_count, query_heads * HEAD_WIDTH)
    )
    log_mass = (row_max + jnp.log(row_sum)).transpose(1, 2, 0, 3).reshape(query_heads, row_count)
    mixed = jnp.dot(
        lax.all_gather(attended, "tp", axis=1, tiled=True),
        w_out,
        preferred_element_type=jnp.float32,
    ).astype(jnp.bfloat16)
    return (mixed[None], log_mass[None])


def solution(mesh):
    in_specs = (
        P("dp", "kv", None),
        P(None, "tp"),
        P(None, "tp"),
        P(None, "tp"),
        P(None, "tp"),
        P("dp", "kv", None),
    )
    out_specs = (P("dp", "kv", "tp"), P("dp", "tp", "kv"))
    return jax.shard_map(body, mesh=mesh, in_specs=in_specs, out_specs=out_specs, check_vma=False)
```

profile of v0, /device:TPU:1, one launch (start us, length us, event | category | flops | bytes accessed | tf_op | source)
XLA Modules:
  0.0 116.2 jit_solution(6678006061197199242)
XLA Ops:
  0.7 0.8 broadcast_remainder_fusion
  1.5 0.7 compare_and_fusion.1
  2.2 0.1 select_reduce_fusion
  2.4 0.7 copy.58
  3.1 19.3 %all-to-all-start = ((s32[64,1,1]{2,1,0:T(1,128)}), s32[64,1,1]{2,1,0:T(1,128)S(1)}, u32[]{:S(2)}, u32[]{:S(2)}) async-start(s32[64,1,1]{2,1,0:T(1,128)} %copy.58), calls=%async_computation | async-start | bytes 65536 | tf_op jit(solution)/shard_map/all_to_all | solution.py:39
  22.4 1.5 %fusion.14 = bf16[320,128]{1,0:T(8,128)(2,1)S(1)} fusion(bf16[2048,128]{1,0:T(8,128)(2,1)} %param.8, bf16[1,320,2048]{2,1,0:T(8,128)(2,1)S(1)} %copy-done), kind=kOutput, calls=%fused_computation.20 | convolution fusion | flops 167813120 | bytes 1916928 | tf_op jit(solution)/shard_map/dot_general | solution.py:24
  23.9 0.5 fusion.17
  24.5 11.3 %all-to-all-done = s32[64,1,1]{2,1,0:T(1,128)S(1)} async-done(((s32[64,1,1]{2,1,0:T(1,128)}), s32[64,1,1]{2,1,0:T(1,128)S(1)}, u32[]{:S(2)}, u32[]{:S(2)}) %all-to-all-start) | async-done | bytes 288 | tf_op jit(solution)/shard_map/all_to_all | solution.py:39
  35.8 1.2 %maximum_reduce_fusion = s32[64]{0:T(128)S(1)} fusion(s32[64,1,1]{2,1,0:T(1,128)S(1)} %all-to-all-done), kind=kLoop, calls=%fused_computation.41 | loop fusion | flops 64 | bytes 512 | tf_op jit(solution)/shard_map/max | solution.py:41
  37.0 0.6 gather_fusion
  37.6 1.2 %compare_reduce_fusion = pred[64]{0:T(512)(128)(4,1)S(1)} fusion(s32[64,1,1]{2,1,0:T(1,128)S(1)} %all-to-all-done), kind=kLoop, calls=%fused_computation.31 | loop fusion | flops 128 | bytes 320 | tf_op jit(solution)/shard_map/jit(_take)/le | solution.py:41
  38.9 1.2 %broadcast_select_fusion.1 = bf16[64,32,256]{2,1,0:T(8,128)(2,1)} fusion(bf16[64,32,256]{2,1,0:T(8,128)(2,1)S(1)} %gather_fusion, pred[64]{0:T(512)(128)(4,1)S(1)} %compare_reduce_fusion), kind=kLoop, calls=%fused_computation.24 | loop fusion | flops 524288 | bytes 2097216 | tf_op jit(solution)/shard_map/jit(_take)/select_n | solution.py:41
  40.1 5.6 %all-to-all-start.1 = ((bf16[64,32,256]{2,1,0:T(8,128)(2,1)}), bf16[64,32,256]{2,1,0:T(8,128)(2,1)}, u32[]{:S(2)}, u32[]{:S(2)}) async-start(bf16[64,32,256]{2,1,0:T(8,128)(2,1)} %broadcast_select_fusion.1), calls=%async_computation.1 | async-start | bytes 2097152 | tf_op jit(solution)/shard_map/all_to_all | solution.py:42
  45.9 0.1 reshape.281
  45.9 0.1 broadcast_in_dim.68
  46.0 0.1 and.100
  46.2 0.1 add.152
  46.3 0.1 add.154
  46.4 0.5 fusion.9
  47.1 0.2 compare_and_fusion
  47.3 49.6 %all-to-all-done.1 = bf16[64,32,256]{2,1,0:T(8,128)(2,1)} async-done(((bf16[64,32,256]{2,1,0:T(8,128)(2,1)}), bf16[64,32,256]{2,1,0:T(8,128)(2,1)}, u32[]{:S(2)}, u32[]{:S(2)}) %all-to-all-start.1) | async-done | bytes 1048608 | tf_op jit(solution)/shard_map/all_to_all | solution.py:42
  96.9 1.3 %pad_maximum_fusion = bf16[74,32,256]{2,1,0:T(8,128)(2,1)S(1)} fusion(bf16[10,32,256]{2,1,0:T(8,128)(2,1)S(1)} %bitcast.114, bf16[64,32,256]{2,1,0:T(8,128)(2,1)} %all-to-all-done.1), kind=kLoop, calls=%fused_computation.15 | loop fusion | flops 606208 | bytes 2424832 | tf_op jit(solution)/shard_map/concatenate | solution.py:43
  98.3 2.5 %gather_fusion.1 = bf16[160,32,256]{2,1,0:T(8,128)(2,1)} fusion(bf16[74,32,256]{2,1,0:T(8,128)(2,1)S(1)} %pad_maximum_fusion, s32[1024]{0:T(1024)S(1)} %pad_clamp_fusion), kind=kCustom, calls=%fused_computation.1 | custom fusion | bytes 5243520 | tf_op jit(solution)/shard_map/jit(_take)/gather | solution.py:45
  100.8 2.1 %broadcast_select_fusion = bf16[10,16,32,256]{3,2,1,0:T(8,128)(2,1)S(1)} fusion(bf16[10,16,32,256]{3,2,1,0:T(8,128)(2,1)} %bitcast.115, pred[10,16]{1,0:T(8,128)(4,1)S(1)} %get-tuple-element.2), kind=kLoop, calls=%fused_computation.2 | loop fusion | flops 1310720 | bytes 5243040 | tf_op jit(solution)/shard_map/jit(_take)/select_n | solution.py:45
  102.8 1.5 %fusion.37 = (bf16[10,16,32,128]{3,2,1,0:T(8,128)(2,1)S(1)}, bf16[10,16,32,128]{3,2,1,0:T(8,128)(2,1)}) fusion(bf16[10,16,32,256]{3,2,1,0:T(8,128)(2,1)S(1)} %broadcast_select_fusion), kind=kLoop, calls=%fused_computation.71 | loop fusion | bytes 5242880 | tf_op jit(solution)/shard_map/slice | solution.py:46
  104.3 0.7 fusion.38
  105.0 0.5 fusion.12
  105.5 0.7 broadcast_in_dim_reshape.2
  106.2 1.8 %fusion.21 = bf16[10,32,1,2,128]{4,1,3,0,2:T(8,128)(2,1)S(1)} fusion(bf16[10,512,128,1]{2,1,3,0:T(8,128)(2,1)} %bitcast.117, f32[10,1,2,32,512]{4,3,2,0,1:T(8,128)S(1)} %get-tuple-element.11, f32[10,2,32]{2,1,0:T(2,128)S(1)} %get-tuple-element.10, f32[10,32,2]{1,2,0:T(2,128)S(1)} %bitcast.120), kind=kOutput, calls=%fused_computation.23 | convolution fusion | flops 84705280 | bytes 2790400 | tf_op jit(solution)/shard_map/bkgts,bskd->btkgd/dot_general | solution.py:71
  107.9 0.1 copy.64
  108.1 6.7 %all_gather.3 = bf16[320,512]{1,0:T(8,128)(2,1)S(1)} all-gather(bf16[320,256]{1,0:T(8,128)(2,1)S(1)} %bitcast.119), channel_id=1, replica_groups=mesh['dp'=4,'kv'=64,'tp'=2] {'tp'}, dimensions={1}, use_global_device_ids=true | all-gather | bytes 491520 | tf_op jit(solution)/shard_map/all_gather | solution.py:81
  114.8 1.3 %fusion.8 = bf16[1,320,1024]{2,1,0:T(8,128)(2,1)} fusion(bf16[320,512]{1,0:T(8,128)(2,1)S(1)} %all_gather.3, bf16[512,1024]{1,0:T(8,128)(2,1)S(1)} %copy-done.1), kind=kOutput, calls=%fused_computation.14 | convolution fusion | flops 335872000 | bytes 2031616 | tf_op jit(solution)/shard_map/dot_general | solution.py:80
  (27 shorter events, 0.4 us)
Async XLA Ops:
  0.6 21.7 %copy-start = (bf16[1,320,2048]{2,1,0:T(8,128)(2,1)S(1)}, bf16[1,320,2048]{2,1,0:T(8,128)(2,1)}, u32[]{:S(2)}) copy-start(bf16[1,320,2048]{2,1,0:T(8,128)(2,1)} %param.6) | copy-start | bytes 3932164
  0.6 23.3 %copy-start.2 = (bf16[2048,128]{1,0:T(8,128)(2,1)S(1)}, bf16[2048,128]{1,0:T(8,128)(2,1)}, u32[]{:S(2)}) copy-start(bf16[2048,128]{1,0:T(8,128)(2,1)} %param.9) | copy-start | bytes 1572868
  3.1 32.7 %all-to-all-start = ((s32[64,1,1]{2,1,0:T(1,128)}), s32[64,1,1]{2,1,0:T(1,128)S(1)}, u32[]{:S(2)}, u32[]{:S(2)}) async-start(s32[64,1,1]{2,1,0:T(1,128)} %copy.58), calls=%async_computation | async-start | bytes 65536 | tf_op jit(solution)/shard_map/all_to_all | solution.py:39
  40.1 5.7 %copy-start.3 = (s32[1,10,16]{2,0,1:T(1,128)S(1)}, s32[1,10,16]{2,0,1:T(1,128)}, u32[]{:S(2)}) copy-start(s32[1,10,16]{2,0,1:T(1,128)} %param.11) | copy-start | bytes 1924
  40.1 6.3 %copy-start.4 = (bf16[2048,256]{1,0:T(8,128)(2,1)S(1)}, bf16[2048,256]{1,0:T(8,128)(2,1)}, u32[]{:S(2)}) copy-start(bf16[2048,256]{1,0:T(8,128)(2,1)} %param.7) | copy-start | bytes 3145732
  40.1 56.9 %all-to-all-start.1 = ((bf16[64,32,256]{2,1,0:T(8,128)(2,1)}), bf16[64,32,256]{2,1,0:T(8,128)(2,1)}, u32[]{:S(2)}, u32[]{:S(2)}) async-start(bf16[64,32,256]{2,1,0:T(8,128)(2,1)} %broadcast_select_fusion.1), calls=%async_computation.1 | async-start | bytes 2097152 | tf_op jit(solution)/shard_map/all_to_all | solution.py:42
  107.9 6.9 %copy-start.1 = (bf16[512,1024]{1,0:T(8,128)(2,1)S(1)}, bf16[512,1024]{1,0:T(8,128)(2,1)}, u32[]{:S(2)}) copy-start(bf16[512,1024]{1,0:T(8,128)(2,1)} %param.10) | copy-start | bytes 3145732
where the time goes:
time: 117 us; the launch traced here: 116 us
  waiting for transfers between devices  60.9 us (52%)
  starting transfers between devices  24.9 us (21%)
  other arithmetic  9.62 us (8%)
  local copies, waits for them, and re-layouts  6.76 us (6%)
  blocking collectives  6.68 us (6%)
  matrix products  6.38 us (5%)
    all_to_all x1, waiting for transfers between devices, body(): lax.all_to_all(replies, 'kv', split_axis=0, concat_axis=0, tiled=True)  49.6 us
    all_to_all x1, starting transfers between devices, body(): lax.all_to_all(wanted, 'kv', split_axis=0, concat_axis=0, tiled=True)  19.3 us
    all_to_all x1, waiting for transfers between devices, body(): lax.all_to_all(wanted, 'kv', split_axis=0, concat_axis=0, tiled=True)  11.3 us
    all_gather x1, blocking collectives, body(): lax.all_gather(attended, 'tp', axis=1, tiled=True)  6.68 us
    all_to_all x1, starting transfers between devices, body(): lax.all_to_all(replies, 'kv', split_axis=0, concat_axis=0, tiled=True)  5.64 us
    gather x1, local copies, waits for them, and re-layouts, body(): picked = jnp.take(block_table, lookup, axis=0)  2.48 us
  transfers between devices with their start and end apart: 2, of which 2 were waited for; matrix products, arithmetic and copies ran while one was open for 3% of the time, Pallas kernels for 0%

commit v1 on v0

--- a/solution.py
+++ b/solution.py
@@ -4,6 +4,14 @@
 from jax.sharding import PartitionSpec as P
 
 HEAD_WIDTH = 128
+
+
+def turn_chunk(mat):
+    shares = lax.axis_size("tp")
+    queue = []
+    for w in range(mat.ndim):
+        queue.append(shares if w == 1 else 1)
+    return lax.all_to_all(jnp.tile(mat, queue), "tp", concat_axis=1, split_axis=1, tiled=True)
 
 
 def body(tokens, w_query, key_weight, value_weight, w_out, chosen):
@@ -77,11 +85,9 @@
         .reshape(row_count, query_heads * HEAD_WIDTH)
     )
     log_mass = (row_max + jnp.log(row_sum)).transpose(1, 2, 0, 3).reshape(query_heads, row_count)
-    mixed = jnp.dot(
-        lax.all_gather(attended, "tp", axis=1, tiled=True),
-        w_out,
-        preferred_element_type=jnp.float32,
-    ).astype(jnp.bfloat16)
+    mixed = jnp.dot(turn_chunk(attended), w_out, preferred_element_type=jnp.float32).astype(
+        jnp.bfloat16
+    )
     return (mixed[None], log_mass[None])
 
 

time: 117 us -> 119 us (1.017)
  blocking collectives: 6.68 us -> 8.64 us
    all_to_all x0 -> x1, blocking collectives: none -> 8.64 us  [turn_chunk(): lax.all_to_all(jnp.tile(mat, queue), 'tp', concat_axis=1, split_axis=1, t...]
    all_gather x1 -> x0, blocking collectives: 6.68 us -> none  [body(): lax.all_gather(attended, 'tp', axis=1, tiled=True)]
where the time goes in v1:
time: 119 us; the launch traced here: 118 us
  waiting for transfers between devices  60.9 us (51%)
  starting transfers between devices  24.9 us (21%)
  other arithmetic  9.62 us (8%)
  blocking collectives  8.64 us (7%)
  local copies, waits for them, and re-layouts  6.8 us (6%)
  matrix products  6.38 us (5%)
    all_to_all x1, waiting for transfers between devices, body(): lax.all_to_all(replies, 'kv', split_axis=0, concat_axis=0, tiled=True)  49.6 us
    all_to_all x1, starting transfers between devices, body(): lax.all_to_all(wanted, 'kv', split_axis=0, concat_axis=0, tiled=True)  19.3 us
    all_to_all x1, waiting for transfers between devices, body(): lax.all_to_all(wanted, 'kv', split_axis=0, concat_axis=0, tiled=True)  11.3 us
    all_to_all x1, blocking collectives, turn_chunk(): lax.all_to_all(jnp.tile(mat, queue), 'tp', concat_axis=1, split_axis=1, t...  8.64 us
    all_to_all x1, starting transfers between devices, body(): lax.all_to_all(replies, 'kv', split_axis=0, concat_axis=0, tiled=True)  5.64 us
    gather x1, local copies, waits for them, and re-layouts, body(): picked = jnp.take(block_table, lookup, axis=0)  2.48 us
  transfers between devices with their start and end apart: 2, of which 2 were waited for; matrix products, arithmetic and copies ran while one was open for 3% of the time, Pallas kernels for 0%

profile of v1, /device:TPU:1, one launch (start us, length us, event | category | flops | bytes accessed | tf_op | source)
XLA Modules:
  0.0 118.2 jit_solution(7122992352431941331)
XLA Ops:
  0.7 0.8 broadcast_remainder_fusion
  1.5 0.7 compare_and_fusion.1
  2.2 0.1 select_reduce_fusion
  2.4 0.7 copy.59
  3.1 19.3 %all-to-all-start = ((s32[64,1,1]{2,1,0:T(1,128)}), s32[64,1,1]{2,1,0:T(1,128)S(1)}, u32[]{:S(2)}, u32[]{:S(2)}) async-start(s32[64,1,1]{2,1,0:T(1,128)} %copy.59), calls=%async_computation | async-start | bytes 65536 | tf_op jit(solution)/shard_map/all_to_all | solution.py:47
  22.4 1.5 %fusion.14 = bf16[320,128]{1,0:T(8,128)(2,1)S(1)} fusion(bf16[2048,128]{1,0:T(8,128)(2,1)} %param.8, bf16[1,320,2048]{2,1,0:T(8,128)(2,1)S(1)} %copy-done), kind=kOutput, calls=%fused_computation.20 | convolution fusion | flops 167813120 | bytes 1916928 | tf_op jit(solution)/shard_map/dot_general | solution.py:32
  23.9 0.5 fusion.17
  24.5 11.3 %all-to-all-done = s32[64,1,1]{2,1,0:T(1,128)S(1)} async-done(((s32[64,1,1]{2,1,0:T(1,128)}), s32[64,1,1]{2,1,0:T(1,128)S(1)}, u32[]{:S(2)}, u32[]{:S(2)}) %all-to-all-start) | async-done | bytes 288 | tf_op jit(solution)/shard_map/all_to_all | solution.py:47
  35.8 1.2 %maximum_reduce_fusion = s32[64]{0:T(128)S(1)} fusion(s32[64,1,1]{2,1,0:T(1,128)S(1)} %all-to-all-done), kind=kLoop, calls=%fused_computation.41 | loop fusion | flops 64 | bytes 512 | tf_op jit(solution)/shard_map/max | solution.py:49
  37.0 0.6 gather_fusion
  37.6 1.2 %compare_reduce_fusion = pred[64]{0:T(512)(128)(4,1)S(1)} fusion(s32[64,1,1]{2,1,0:T(1,128)S(1)} %all-to-all-done), kind=kLoop, calls=%fused_computation.31 | loop fusion | flops 128 | bytes 320 | tf_op jit(solution)/shard_map/jit(_take)/le | solution.py:49
  38.9 1.2 %broadcast_select_fusion.1 = bf16[64,32,256]{2,1,0:T(8,128)(2,1)} fusion(bf16[64,32,256]{2,1,0:T(8,128)(2,1)S(1)} %gather_fusion, pred[64]{0:T(512)(128)(4,1)S(1)} %compare_reduce_fusion), kind=kLoop, calls=%fused_computation.24 | loop fusion | flops 524288 | bytes 2097216 | tf_op jit(solution)/shard_map/jit(_take)/select_n | solution.py:49
  40.1 5.6 %all-to-all-start.1 = ((bf16[64,32,256]{2,1,0:T(8,128)(2,1)}), bf16[64,32,256]{2,1,0:T(8,128)(2,1)}, u32[]{:S(2)}, u32[]{:S(2)}) async-start(bf16[64,32,256]{2,1,0:T(8,128)(2,1)} %broadcast_select_fusion.1), calls=%async_computation.1 | async-start | bytes 2097152 | tf_op jit(solution)/shard_map/all_to_all | solution.py:50
  45.9 0.1 reshape.284
  45.9 0.1 broadcast_in_dim.68
  46.0 0.1 and.100
  46.2 0.1 add.152
  46.3 0.1 add.154
  46.4 0.5 fusion.9
  47.1 0.2 compare_and_fusion
  47.3 49.6 %all-to-all-done.1 = bf16[64,32,256]{2,1,0:T(8,128)(2,1)} async-done(((bf16[64,32,256]{2,1,0:T(8,128)(2,1)}), bf16[64,32,256]{2,1,0:T(8,128)(2,1)}, u32[]{:S(2)}, u32[]{:S(2)}) %all-to-all-start.1) | async-done | bytes 1048608 | tf_op jit(solution)/shard_map/all_to_all | solution.py:50
  96.9 1.3 %pad_maximum_fusion = bf16[74,32,256]{2,1,0:T(8,128)(2,1)S(1)} fusion(bf16[10,32,256]{2,1,0:T(8,128)(2,1)S(1)} %bitcast.116, bf16[64,32,256]{2,1,0:T(8,128)(2,1)} %all-to-all-done.1), kind=kLoop, calls=%fused_computation.15 | loop fusion | flops 606208 | bytes 2424832 | tf_op jit(solution)/shard_map/concatenate | solution.py:51
  98.3 2.5 %gather_fusion.1 = bf16[160,32,256]{2,1,0:T(8,128)(2,1)} fusion(bf16[74,32,256]{2,1,0:T(8,128)(2,1)S(1)} %pad_maximum_fusion, s32[1024]{0:T(1024)S(1)} %pad_clamp_fusion), kind=kCustom, calls=%fused_computation.1 | custom fusion | bytes 5243520 | tf_op jit(solution)/shard_map/jit(_take)/gather | solution.py:53
  100.8 2.1 %broadcast_select_fusion = bf16[10,16,32,256]{3,2,1,0:T(8,128)(2,1)S(1)} fusion(bf16[10,16,32,256]{3,2,1,0:T(8,128)(2,1)} %bitcast.117, pred[10,16]{1,0:T(8,128)(4,1)S(1)} %get-tuple-element.2), kind=kLoop, calls=%fused_computation.2 | loop fusion | flops 1310720 | bytes 5243040 | tf_op jit(solution)/shard_map/jit(_take)/select_n | solution.py:53
  102.8 1.5 %fusion.37 = (bf16[10,16,32,128]{3,2,1,0:T(8,128)(2,1)S(1)}, bf16[10,16,32,128]{3,2,1,0:T(8,128)(2,1)}) fusion(bf16[10,16,32,256]{3,2,1,0:T(8,128)(2,1)S(1)} %broadcast_select_fusion), kind=kLoop, calls=%fused_computation.71 | loop fusion | bytes 5242880 | tf_op jit(solution)/shard_map/slice | solution.py:54
  104.3 0.7 fusion.38
  105.0 0.5 fusion.12
  105.5 0.7 broadcast_in_dim_reshape.2
  106.2 1.8 %fusion.21 = bf16[10,32,1,2,128]{4,1,3,0,2:T(8,128)(2,1)S(1)} fusion(bf16[10,512,128,1]{2,1,3,0:T(8,128)(2,1)} %bitcast.119, f32[10,1,2,32,512]{4,3,2,0,1:T(8,128)S(1)} %get-tuple-element.11, f32[10,2,32]{2,1,0:T(2,128)S(1)} %get-tuple-element.10, f32[10,32,2]{1,2,0:T(2,128)S(1)} %bitcast.124), kind=kOutput, calls=%fused_computation.23 | convolution fusion | flops 84705280 | bytes 2790400 | tf_op jit(solution)/shard_map/bkgts,bskd->btkgd/dot_general | solution.py:79
  107.9 0.1 copy.65
  108.2 8.6 %all_to_all.23 = bf16[320,2,256]{2,0,1:T(8,128)(2,1)S(1)} all-to-all(bf16[320,2,256]{2,0,1:T(8,128)(2,1)S(1)} %tile.9), channel_id=1, replica_groups=mesh['dp'=4,'kv'=64,'tp'=2] {'tp'}, dimensions={1} | all-to-all | bytes 655360 | tf_op jit(solution)/shard_map/all_to_all | solution.py:14
  116.8 1.3 %fusion.8 = bf16[1,320,1024]{2,1,0:T(8,128)(2,1)} fusion(bf16[320,512]{1,0:T(8,128)(2,1)S(1)} %bitcast.120, bf16[512,1024]{1,0:T(8,128)(2,1)S(1)} %copy-done.1), kind=kOutput, calls=%fused_computation.14 | convolution fusion | flops 335872000 | bytes 2031616 | tf_op jit(solution)/shard_map/dot_general | solution.py:88
  (29 shorter events, 0.5 us)
Async XLA Ops:
  0.6 21.7 %copy-start = (bf16[1,320,2048]{2,1,0:T(8,128)(2,1)S(1)}, bf16[1,320,2048]{2,1,0:T(8,128)(2,1)}, u32[]{:S(2)}) copy-start(bf16[1,320,2048]{2,1,0:T(8,128)(2,1)} %param.6) | copy-start | bytes 3932164
  0.6 23.3 %copy-start.2 = (bf16[2048,128]{1,0:T(8,128)(2,1)S(1)}, bf16[2048,128]{1,0:T(8,128)(2,1)}, u32[]{:S(2)}) copy-start(bf16[2048,128]{1,0:T(8,128)(2,1)} %param.9) | copy-start | bytes 1572868
  3.1 32.7 %all-to-all-start = ((s32[64,1,1]{2,1,0:T(1,128)}), s32[64,1,1]{2,1,0:T(1,128)S(1)}, u32[]{:S(2)}, u32[]{:S(2)}) async-start(s32[64,1,1]{2,1,0:T(1,128)} %copy.59), calls=%async_computation | async-start | bytes 65536 | tf_op jit(solution)/shard_map/all_to_all | solution.py:47
  40.1 5.7 %copy-start.3 = (s32[1,10,16]{2,0,1:T(1,128)S(1)}, s32[1,10,16]{2,0,1:T(1,128)}, u32[]{:S(2)}) copy-start(s32[1,10,16]{2,0,1:T(1,128)} %param.11) | copy-start | bytes 1924
  40.1 6.3 %copy-start.4 = (bf16[2048,256]{1,0:T(8,128)(2,1)S(1)}, bf16[2048,256]{1,0:T(8,128)(2,1)}, u32[]{:S(2)}) copy-start(bf16[2048,256]{1,0:T(8,128)(2,1)} %param.7) | copy-start | bytes 3145732
  40.1 56.9 %all-to-all-start.1 = ((bf16[64,32,256]{2,1,0:T(8,128)(2,1)}), bf16[64,32,256]{2,1,0:T(8,128)(2,1)}, u32[]{:S(2)}, u32[]{:S(2)}) async-start(bf16[64,32,256]{2,1,0:T(8,128)(2,1)} %broadcast_select_fusion.1), calls=%async_computation.1 | async-start | bytes 2097152 | tf_op jit(solution)/shard_map/all_to_all | solution.py:50
  107.9 8.9 %copy-start.1 = (bf16[512,1024]{1,0:T(8,128)(2,1)S(1)}, bf16[512,1024]{1,0:T(8,128)(2,1)}, u32[]{:S(2)}) copy-start(bf16[512,1024]{1,0:T(8,128)(2,1)} %param.10) | copy-start | bytes 3145732
